TPU v7x, 32 devices: a whole 2x2x4 slice. The times are simulated.
32 devices in a mesh: grp: 2 (over x), ep: 16 (over z, y, core).
Axes of the slice: x: 2, y: 2, z: 4, core: 2. Of those that a mesh axis runs over, the one named last changes fastest.
Arguments:
- queries: bfloat16 [32, 8, 128], P(('grp', 'ep')), parts along dimension 0, may hold values from -400 to 400
- fresh_token_key: bfloat16 [32, 2, 128], P(('grp', 'ep')), parts along dimension 0, may hold values from -6 to 6
- value_new: bfloat16 [32, 2, 128], P(('grp', 'ep')), parts along dimension 0, may hold values from -6 to 6
- forget_logit: float32 [32, 8], P(('grp', 'ep')), parts along dimension 0, may hold values from -8 to 8
- cache_keys: bfloat16 [32, 2, 4096, 128], P(('grp', 'ep')), parts along dimension 0, may hold values from -12 to 12
- cache_values: bfloat16 [32, 2, 4096, 128], P(('grp', 'ep')), parts along dimension 0, may hold values from -6 to 6
- cache_cumlog: float32 [32, 8, 4096], P(('grp', 'ep')), parts along dimension 0, may hold values from -572 to 0
- lengths: int32 [32], P(('grp', 'ep')), parts along dimension 0, may hold values from 1024 to 4096
- residual: bfloat16 [32, 2048], P('grp', 'ep'), parts along dimension 0, may hold values from -6 to 6
- out_weight: bfloat16 [1024, 2048], P(None, 'ep'), may hold values from -0.1875 to 0.1875
- norm_gain: float32 [2048], replicated, may hold values from 0.1 to 1.9
- expert_gate: bfloat16 [16, 704, 2048], P('ep'), may hold values from -0.125 to 0.125
- expert_up: bfloat16 [16, 704, 2048], P('ep'), may hold values from -0.125 to 0.125
- expert_down: bfloat16 [16, 704, 2048], P('ep'), may hold values from -0.21875 to 0.21875
- shared_gate: bfloat16 [1408, 2048], P('ep'), may hold values from -0.125 to 0.125
- shared_up: bfloat16 [1408, 2048], P('ep'), may hold values from -0.125 to 0.125
- shared_down: bfloat16 [1408, 2048], P(None, 'ep'), may hold values from -0.15625 to 0.15625
- routes: int32 [32, 6], P('grp'), parts along dimension 0, may hold values from 0 to 15, all different within a row; in each aligned block of 16 rows (0 to 15, 16 to 31, ...) at most 12 rows name the same one
- route_scores: float32 [32, 6], P('grp'), parts along dimension 0, may hold values from 0.05 to 1
Outputs:
- updated: bfloat16 [32, 2048], P('grp', 'ep'), parts along dimension 0
There are 2 independent parts, one for each index of `grp`. A program takes and returns all parts, laid end to end along the dimension named above; an argument that names none is the same for every part. Nothing has to cross between parts.
Inputs may be any that keep to these rules, and one draw needn't show every extreme that they name: `routes`: each row names 6 different experts; no expert is named by more than 12 rows of a part, a bound that some block reaches.
All inputs are finite; a program needn't handle non-finite values.
Results may differ from a plain program's by a relative error of at most 0.0068.
Values may be sent and summed in bfloat16 or wider, within the bound.
A program may use at most 64 MiB of HBM per device.

v0:
```python
import functools

import jax
import jax.numpy as jnp
from jax import lax
from jax.experimental import pallas as pl
from jax.experimental.pallas import tpu as pltpu
from jax.sharding import PartitionSpec as P

norm_eps = 1e-06
routed_scale = 2.5
contract_last = (((1,), (1,)), ((), ()))
LANES = 128
f32 = jnp.float32
bf16 = jnp.bfloat16


def dot_t(a, b):
    return lax.dot_general(a, b, contract_last, preferred_element_type=f32)


def join_lanes(blocks, width):
    if width % LANES == 0:
        return jnp.concatenate([b.astype(bf16) for b in blocks], axis=1)
    rows = blocks[0].shape[0]
    total = len(blocks) * width
    lane = lax.broadcasted_iota(jnp.int32, (rows, LANES), 1)
    pieces = [jnp.zeros((rows, LANES), f32) for _ in range(-(-total // LANES))]
    for k, block in enumerate(blocks):
        at, shift = divmod(k * width, LANES)
        moved = jnp.where(lane < width, block.astype(f32), 0.0)
        if shift:
            moved = pltpu.roll(moved, shift, 1)
        if shift + width <= LANES:
            pieces[at] = pieces[at] + moved
        else:
            pieces[at] = pieces[at] + jnp.where(lane >= shift, moved, 0.0)
            pieces[at + 1] = pieces[at + 1] + jnp.where(lane < shift, moved, 0.0)
    return jnp.concatenate([p.astype(bf16) for p in pieces], axis=1)[:, :total]


def widen(block):
    rows, width = block.shape
    short = -width % LANES
    if not short:
        return block
    return jnp.concatenate([block, jnp.zeros((rows, short), block.dtype)], axis=1)


def layer(
    n,
    lengths_ref,
    q_ref,
    fresh_ref,
    vnew_ref,
    forget_ref,
    residual_ref,
    gain_ref,
    routes_ref,
    route_scores_ref,
    keys_hbm,
    values_hbm,
    cumlog_hbm,
    out_w_hbm,
    gate_hbm,
    up_hbm,
    down_hbm,
    sgate_hbm,
    sup_hbm,
    sdown_hbm,
    out_ref,
    keys,
    values,
    cumlog,
    out_w,
    gate_w,
    up_w,
    down_w,
    sgate_w,
    sup_w,
    sdown_w,
    scores,
    att_buf,
    att_wide,
    stream_buf,
    mid_buf,
    eo_src,
    eo_buf,
    load_sem,
    key_sem,
    value_sem,
    send_sem,
    recv_sem,
):
    me = lax.axis_index("ep")
    heads, head_size = q_ref.shape[1:]
    key_heads, span = keys.shape[:2]
    groups = heads // key_heads
    rows, width = residual_ref.shape
    model = gate_w.shape[1]
    shared_width = sgate_w.shape[0]
    chunks = key_sem.shape[0]
    chunk = span // chunks

    def key_copy(c):
        part = pl.ds(c * chunk, chunk)
        return pltpu.make_async_copy(keys_hbm.at[0, :, part], keys.at[:, part], key_sem.at[c])

    def value_copy(c):
        part = pl.ds(c * chunk, chunk)
        return pltpu.make_async_copy(values_hbm.at[0, :, part], values.at[:, part], value_sem.at[c])

    cumlog_copy = pltpu.make_async_copy(cumlog_hbm.at[0], cumlog, load_sem.at[0])
    out_w_copy = pltpu.make_async_copy(out_w_hbm, out_w, load_sem.at[1])
    sgate_copy = pltpu.make_async_copy(sgate_hbm, sgate_w, load_sem.at[2])
    sup_copy = pltpu.make_async_copy(sup_hbm, sup_w, load_sem.at[3])
    gate_copy = pltpu.make_async_copy(gate_hbm.at[0], gate_w, load_sem.at[4])
    up_copy = pltpu.make_async_copy(up_hbm.at[0], up_w, load_sem.at[5])
    down_copy = pltpu.make_async_copy(down_hbm.at[0], down_w, load_sem.at[6])
    sdown_copy = pltpu.make_async_copy(sdown_hbm, sdown_w, load_sem.at[7])

    cumlog_copy.start()
    for c in range(chunks):
        key_copy(c).start()
    for c in range(chunks):
        value_copy(c).start()
    out_w_copy.start()

    barrier = pltpu.get_barrier_semaphore()

    def greet(i, carry):
        pl.semaphore_signal(barrier, inc=1, device_id={"ep": lax.rem(me + i, n)})
        return carry

    lax.fori_loop(1, n, greet, 0)

    def remote(phase, src, dst, peer, slot):
        return pltpu.make_async_remote_copy(
            src_ref=src,
            dst_ref=dst,
            send_sem=send_sem.at[phase, peer],
            recv_sem=recv_sem.at[phase, slot],
            device_id={"ep": peer},
        )

    def spread(phase, buf):
        def one(i, carry):
            peer = lax.rem(me + i, n)
            remote(phase, buf.at[me], buf.at[me], peer, me).start()
            return carry

        lax.fori_loop(1, n, one, 0)

    def arrive(phase, buf):
        def one(i, carry):
            peer = lax.rem(me + i, n)
            remote(phase, buf.at[peer], buf.at[peer], peer, peer).wait_recv()
            return carry

        lax.fori_loop(1, n, one, 0)

    def sent(phase, buf):
        def one(i, carry):
            peer = lax.rem(me + i, n)
            remote(phase, buf.at[peer], buf.at[peer], peer, peer).wait_send()
            return carry

        lax.fori_loop(1, n, one, 0)

    inv_root = head_size ** (-0.5)
    length = lengths_ref[0]
    q = q_ref[0]
    head_row = lax.broadcasted_iota(jnp.int32, (heads, head_size), 0)
    q_wide = jnp.concatenate(
        [jnp.where(head_row // groups == k, q, jnp.zeros_like(q)) for k in range(key_heads)], axis=1
    )
    fresh, vnew = fresh_ref[0].astype(f32), vnew_ref[0].astype(f32)
    own_key, own_value = fresh[0:1], vnew[0:1]
    for k in range(1, key_heads):
        own_key = jnp.where(head_row // groups == k, fresh[k : k + 1], own_key)
        own_value = jnp.where(head_row // groups == k, vnew[k : k + 1], own_value)
    own_score = jnp.sum(q.astype(f32) * own_key, axis=1, keepdims=True) * inv_root
    eye = lax.broadcasted_iota(jnp.int32, (heads, heads), 0) == lax.broadcasted_iota(
        jnp.int32, (heads, heads), 1
    )
    forget = jnp.sum(jnp.where(eye, forget_ref[...], 0.0), axis=1, keepdims=True)
    log_gate = jnp.minimum(forget, 0.0) - jnp.log1p(jnp.exp(-jnp.abs(forget)))

    cumlog_copy.wait()
    position = lax.broadcasted_iota(jnp.int32, (heads, span), 1)
    latest = (
        jnp.sum(jnp.where(position == length - 1, cumlog[...], 0.0), axis=1, keepdims=True)
        + log_gate
    )
    place = lax.broadcasted_iota(jnp.int32, (heads, chunk), 1)
    top = own_score
    for c in range(chunks):
        key_copy(c).wait()
        part = slice(c * chunk, (c + 1) * chunk)
        both = jnp.concatenate([keys[k, part] for k in range(key_heads)], axis=1)
        score = dot_t(q_wide, both) * inv_root + latest - cumlog[:, part]
        score = jnp.where(place + c * chunk < length, score, -jnp.inf)
        scores[:, part] = score
        top = jnp.maximum(top, jnp.max(score, axis=1, keepdims=True))

    sgate_copy.start()
    sup_copy.start()
    gate_copy.start()
    up_copy.start()
    down_copy.start()
    sdown_copy.start()

    own_weight = jnp.exp(own_score - top)
    denominator = own_weight
    weighted = jnp.zeros((heads, key_heads * head_size), f32)
    for c in range(chunks):
        value_copy(c).wait()
        part = slice(c * chunk, (c + 1) * chunk)
        weight = jnp.exp(scores[:, part] - top)
        denominator = denominator + jnp.sum(weight, axis=1, keepdims=True)
        both = jnp.concatenate([values[k, part] for k in range(key_heads)], axis=1)
        weighted = weighted + jnp.dot(weight.astype(bf16), both, preferred_element_type=f32)
    mine = weighted[:, :head_size]
    for k in range(1, key_heads):
        mine = jnp.where(
            head_row // groups == k, weighted[:, k * head_size : (k + 1) * head_size], mine
        )
    numerator = mine + own_weight.astype(bf16).astype(f32) * own_value
    att_buf[me] = (numerator / denominator).astype(bf16)

    pl.semaphore_wait(barrier, n - 1)
    spread(0, att_buf)

    route_scores = route_scores_ref[...]
    gate_weights = (
        route_scores / jnp.sum(route_scores, axis=1, keepdims=True) * routed_scale
    )
    expert_lane = lax.broadcasted_iota(jnp.int32, (rows, n), 1)
    share = jnp.zeros((rows, n), f32)
    for k in range(routes_ref.shape[1]):
        share = share + jnp.where(
            routes_ref[:, k : k + 1] == expert_lane, gate_weights[:, k : k + 1], 0.0
        )
    out_w_copy.wait()

    arrive(0, att_buf)
    att_wide[...] = att_buf[...].astype(f32).reshape(n * heads, head_size)
    attended = jnp.concatenate(
        [att_wide[pl.ds(h, n, stride=heads), :].astype(bf16) for h in range(heads)], axis=1
    )
    mixed = jnp.dot(attended, out_w[...], preferred_element_type=f32)
    stream = (residual_ref[...].astype(f32) + mixed).astype(bf16)
    stream_buf[me] = widen(stream)
    spread(1, stream_buf)
    sgate_copy.wait()
    sup_copy.wait()
    gate_copy.wait()
    up_copy.wait()
    arrive(1, stream_buf)

    full = join_lanes([stream_buf[j] for j in range(n)], width).astype(f32)
    inv_rms = lax.rsqrt(jnp.mean(full * full, axis=1, keepdims=True) + norm_eps)
    normed = (full * inv_rms * gain_ref[...]).astype(bf16)

    def hidden_of(gate, up):
        gated = dot_t(normed, gate)
        return (jax.nn.silu(gated) * dot_t(normed, up)).astype(bf16)

    mid_buf[me] = widen(hidden_of(sgate_w[...], sup_w[...]))
    spread(2, mid_buf)

    hidden = hidden_of(gate_w[...], up_w[...])
    down_copy.wait()
    wide = max(width, 2 * LANES)
    per = wide // width
    turns = model // wide

    def send_block(peer):
        remote(3, eo_src.at[peer], eo_buf.at[me], peer, me).start()

    for i in range(turns):
        c = lax.rem(me // per + 1 + i, turns)
        part = pl.ds(pl.multiple_of(c * wide, wide), wide)
        out = jnp.dot(hidden, down_w[:, part], preferred_element_type=f32).astype(bf16)
        for s in range(per):
            peer = c * per + s
            eo_src[peer] = widen(out[:, s * width : (s + 1) * width])
        for s in range(per):
            peer = c * per + s
            if i < turns - 1:
                send_block(peer)
            else:
                pl.when(peer != me)(functools.partial(send_block, peer))
    eo_buf[me] = eo_src[me]

    sdown_copy.wait()
    arrive(2, mid_buf)
    mid = join_lanes([mid_buf[j] for j in range(n)], shared_width)
    total = stream.astype(f32) + jnp.dot(mid, sdown_w[...], preferred_element_type=f32)
    arrive(3, eo_buf)
    for e in range(n):
        total = total + share[:, e : e + 1] * eo_buf[e][:, :width].astype(f32)
    out_ref[...] = total.astype(bf16)

    sent(0, att_buf)
    sent(1, stream_buf)
    sent(2, mid_buf)
    sent(3, eo_buf)


def solution(mesh):
    n = mesh.shape["ep"]

    def on_device(
        queries,
        fresh_token_key,
        value_new,
        forget_logit,
        cache_keys,
        cache_values,
        cache_cumlog,
        lengths,
        residual,
        out_weight,
        norm_gain,
        expert_gate,
        expert_up,
        expert_down,
        shared_gate,
        shared_up,
        shared_down,
        routes,
        route_scores,
    ):
        rows, width = residual.shape
        heads, head_size = queries.shape[1:]
        span = cache_keys.shape[2]
        lanes = -(-width // LANES) * LANES
        mid_lanes = -(-shared_gate.shape[0] // LANES) * LANES
        chunks = 4
        vmem = pl.BlockSpec(memory_space=pltpu.VMEM)
        hbm = pl.BlockSpec(memory_space=pl.ANY)

        def like(a, drop=0):
            return pltpu.VMEM(a.shape[drop:], a.dtype)

        return pl.pallas_call(
            functools.partial(layer, n),
            out_shape=jax.ShapeDtypeStruct((rows, width), bf16),
            in_specs=[pl.BlockSpec(memory_space=pltpu.SMEM)] + [vmem] * 8 + [hbm] * 10,
            out_specs=vmem,
            scratch_shapes=[
                like(cache_keys, 1),
                like(cache_values, 1),
                like(cache_cumlog, 1),
                like(out_weight),
                like(expert_gate, 1),
                like(expert_up, 1),
                like(expert_down, 1),
                like(shared_gate),
                like(shared_up),
                like(shared_down),
                pltpu.VMEM((heads, span), f32),
                pltpu.VMEM((n, heads, head_size), bf16),
                pltpu.VMEM((n * heads, head_size), f32),
                pltpu.VMEM((n, rows, lanes), bf16),
                pltpu.VMEM((n, rows, mid_lanes), bf16),
                pltpu.VMEM((n, rows, lanes), bf16),
                pltpu.VMEM((n, rows, lanes), bf16),
                pltpu.SemaphoreType.DMA((8,)),
                pltpu.SemaphoreType.DMA((chunks,)),
                pltpu.SemaphoreType.DMA((chunks,)),
                pltpu.SemaphoreType.DMA((4, n)),
                pltpu.SemaphoreType.DMA((4, n)),
            ],
            compiler_params=pltpu.CompilerParams(
                collective_id=0, has_side_effects=True, vmem_limit_bytes=48 * 1024 * 1024
            ),
            name="layer",
        )(
            lengths,
            queries,
            fresh_token_key,
            value_new,
            forget_logit,
            residual,
            norm_gain.reshape(1, -1),
            routes,
            route_scores,
            cache_keys,
            cache_values,
            cache_cumlog,
            out_weight,
            expert_gate,
            expert_up,
            expert_down,
            shared_gate,
            shared_up,
            shared_down,
        )

    placed = (
        P(("grp", "ep"), None, None),
        P(("grp", "ep"), None, None),
        P(("grp", "ep"), None, None),
        P(("grp", "ep"), None),
        P(("grp", "ep"), None, None, None),
        P(("grp", "ep"), None, None, None),
        P(("grp", "ep"), None, None),
        P(("grp", "ep")),
        P("grp", "ep"),
        P(None, "ep"),
        P(),
        P("ep", None, None),
        P("ep", None, None),
        P("ep", None, None),
        P("ep", None),
        P("ep", None),
        P(None, "ep"),
        P("grp", None),
        P("grp", None),
    )
    return jax.shard_map(
        on_device, mesh=mesh, in_specs=placed, out_specs=P("grp", "ep"), check_vma=False
    )
```

profile of v0, /device:TPU:0, one launch (start us, length us, event | category | flops | bytes accessed | tf_op | source)
XLA Modules:
  0.0 38.9 jit_solution(1290263653662504500)
XLA Ops:
  0.7 0.8 %copy.20.routes_ref = s32[16,6]{1,0:T(8,128)S(1)} copy(s32[16,6]{0,1:T(8,128)} %param.36) | data formatting | bytes 768 | tf_op args[17]
  1.4 0.8 %copy.21.route_scores_ref = f32[16,6]{1,0:T(8,128)S(1)} copy(f32[16,6]{0,1:T(8,128)} %param.37) | data formatting | bytes 768 | tf_op args[18]
  2.2 0.0 copy-start
  2.2 1.6 %copy-done = bf16[1,2,4096,128]{3,2,1,0:T(8,128)(2,1)S(1)} copy-done((bf16[1,2,4096,128]{3,2,1,0:T(8,128)(2,1)S(1)}, bf16[1,2,4096,128]{3,2,1,0:T(8,128)(2,1)}, u32[]{:S(2)}) %copy-start) | copy-done | bytes 2097176
  3.8 0.0 copy-start.1
  3.8 1.6 %copy-done.1 = bf16[1,2,4096,128]{3,2,1,0:T(8,128)(2,1)S(1)} copy-done((bf16[1,2,4096,128]{3,2,1,0:T(8,128)(2,1)S(1)}, bf16[1,2,4096,128]{3,2,1,0:T(8,128)(2,1)}, u32[]{:S(2)}) %copy-start.1) | copy-done | bytes 2097176
  5.4 0.0 copy-start.2
  5.4 1.0 %copy-done.2 = bf16[88,2048]{1,0:T(8,128)(2,1)S(1)} copy-done((bf16[88,2048]{1,0:T(8,128)(2,1)S(1)}, bf16[88,2048]{1,0:T(8,128)(2,1)}, u32[]{:S(2)}) %copy-start.2) | copy-done | bytes 360472
  6.3 0.0 copy-start.3
  6.3 1.0 %copy-done.3 = bf16[88,2048]{1,0:T(8,128)(2,1)S(1)} copy-done((bf16[88,2048]{1,0:T(8,128)(2,1)S(1)}, bf16[88,2048]{1,0:T(8,128)(2,1)}, u32[]{:S(2)}) %copy-start.3) | copy-done | bytes 360472
  7.3 0.0 copy-start.4
  7.3 1.0 %copy-done.4 = bf16[1408,128]{1,0:T(8,128)(2,1)S(1)} copy-done((bf16[1408,128]{1,0:T(8,128)(2,1)S(1)}, bf16[1408,128]{1,0:T(8,128)(2,1)}, u32[]{:S(2)}) %copy-start.4) | copy-done | bytes 360472
  8.3 0.0 copy-start.5
  8.3 0.9 %copy-done.5 = bf16[1024,128]{1,0:T(8,128)(2,1)S(1)} copy-done((bf16[1024,128]{1,0:T(8,128)(2,1)S(1)}, bf16[1024,128]{1,0:T(8,128)(2,1)}, u32[]{:S(2)}) %copy-start.5) | copy-done | bytes 262168
  9.3 0.0 copy-start.6
  9.3 0.9 %copy-done.6 = f32[1,8,4096]{2,1,0:T(8,128)S(1)} copy-done((f32[1,8,4096]{2,1,0:T(8,128)S(1)}, f32[1,8,4096]{2,1,0:T(8,128)}, u32[]{:S(2)}) %copy-start.6) | copy-done | bytes 131096
  10.2 0.0 copy-start.7
  10.2 0.7 %copy-done.7 = f32[2048]{0:T(1024)S(1)} copy-done((f32[2048]{0:T(1024)S(1)}, f32[2048]{0:T(1024)}, u32[]{:S(2)}) %copy-start.7) | copy-done | bytes 8216
  10.9 0.0 copy-start.8
  10.9 0.7 %copy-done.8 = bf16[16,128]{1,0:T(8,128)(2,1)S(1)} copy-done((bf16[16,128]{1,0:T(8,128)(2,1)S(1)}, bf16[16,128]{1,0:T(8,128)(2,1)}, u32[]{:S(2)}) %copy-start.8) | copy-done | bytes 4120
  11.6 0.0 copy-start.9
  11.6 0.7 %copy-done.9 = bf16[1,8,128]{2,1,0:T(8,128)(2,1)S(1)} copy-done((bf16[1,8,128]{2,1,0:T(8,128)(2,1)S(1)}, bf16[1,8,128]{2,1,0:T(8,128)(2,1)}, u32[]{:S(2)}) %copy-start.9) | copy-done | bytes 2072
  12.2 0.0 copy-start.10
  12.2 0.7 %copy-done.10 = bf16[1,2,128]{2,1,0:T(2,128)(2,1)S(1)} copy-done((bf16[1,2,128]{2,1,0:T(2,128)(2,1)S(1)}, bf16[1,2,128]{2,1,0:T(2,128)(2,1)}, u32[]{:S(2)}) %copy-start.10) | copy-done | bytes 536
  12.9 0.0 copy-start.11
  12.9 0.7 %copy-done.11 = bf16[1,2,128]{2,1,0:T(2,128)(2,1)S(1)} copy-done((bf16[1,2,128]{2,1,0:T(2,128)(2,1)S(1)}, bf16[1,2,128]{2,1,0:T(2,128)(2,1)}, u32[]{:S(2)}) %copy-start.11) | copy-done | bytes 536
  13.6 0.0 copy-start.12
  13.6 0.7 %copy-done.12 = f32[1,8]{1,0:T(1,128)S(1)} copy-done((f32[1,8]{1,0:T(1,128)S(1)}, f32[1,8]{1,0:T(1,128)}, u32[]{:S(2)}) %copy-start.12) | copy-done | bytes 56
  14.2 24.1 %layer.1 = bf16[16,128]{1,0:T(8,128)(2,1)S(1)} custom-call(s32[1]{0:T(128)S(6)} %copy.23.lengths_ref, bf16[1,8,128]{2,1,0:T(8,128)(2,1)S(1)} %copy-done.9, bf16[1,2,128]{2,1,0:T(2,128)(2,1)S(1)} %copy-done.10, bf16[1,2,128]{2,1,0:T(2,128)(2,1)S(1)} %copy-done.11, f32[1,8]{1,0:T(1,128)S(1)} %copy-done.12, bf16[16,128]{1,0:T(8,128)(2,1)S(1)} %copy-done.8, ...), custom_call_target="tpu_custom_call" | custom-call | tf_op jit(solution)/shard_map/layer/pallas_call | solution.py:347
  38.4 0.6 %copy.24 = bf16[16,128]{1,0:T(8,128)(2,1)} copy(bf16[16,128]{1,0:T(8,128)(2,1)S(1)} %layer.1) | data formatting | bytes 8192
Async XLA Ops:
  2.2 1.6 %copy-start = (bf16[1,2,4096,128]{3,2,1,0:T(8,128)(2,1)S(1)}, bf16[1,2,4096,128]{3,2,1,0:T(8,128)(2,1)}, u32[]{:S(2)}) copy-start(bf16[1,2,4096,128]{3,2,1,0:T(8,128)(2,1)} %keys_hbm.1) | copy-start | bytes 6291460
  3.8 1.6 %copy-start.1 = (bf16[1,2,4096,128]{3,2,1,0:T(8,128)(2,1)S(1)}, bf16[1,2,4096,128]{3,2,1,0:T(8,128)(2,1)}, u32[]{:S(2)}) copy-start(bf16[1,2,4096,128]{3,2,1,0:T(8,128)(2,1)} %values_hbm.1) | copy-start | bytes 6291460
  5.4 1.0 %copy-start.2 = (bf16[88,2048]{1,0:T(8,128)(2,1)S(1)}, bf16[88,2048]{1,0:T(8,128)(2,1)}, u32[]{:S(2)}) copy-start(bf16[88,2048]{1,0:T(8,128)(2,1)} %sgate_hbm.1) | copy-start | bytes 1081348
  6.3 1.0 %copy-start.3 = (bf16[88,2048]{1,0:T(8,128)(2,1)S(1)}, bf16[88,2048]{1,0:T(8,128)(2,1)}, u32[]{:S(2)}) copy-start(bf16[88,2048]{1,0:T(8,128)(2,1)} %sup_hbm.1) | copy-start | bytes 1081348
  7.3 1.0 %copy-start.4 = (bf16[1408,128]{1,0:T(8,128)(2,1)S(1)}, bf16[1408,128]{1,0:T(8,128)(2,1)}, u32[]{:S(2)}) copy-start(bf16[1408,128]{1,0:T(8,128)(2,1)} %sdown_hbm.1) | copy-start | bytes 1081348
  8.3 0.9 %copy-start.5 = (bf16[1024,128]{1,0:T(8,128)(2,1)S(1)}, bf16[1024,128]{1,0:T(8,128)(2,1)}, u32[]{:S(2)}) copy-start(bf16[1024,128]{1,0:T(8,128)(2,1)} %out_w_hbm.1) | copy-start | bytes 786436
  9.3 0.9 %copy-start.6 = (f32[1,8,4096]{2,1,0:T(8,128)S(1)}, f32[1,8,4096]{2,1,0:T(8,128)}, u32[]{:S(2)}) copy-start(f32[1,8,4096]{2,1,0:T(8,128)} %cumlog_hbm.1) | copy-start | bytes 393220
  10.2 0.7 %copy-start.7 = (f32[2048]{0:T(1024)S(1)}, f32[2048]{0:T(1024)}, u32[]{:S(2)}) copy-start(f32[2048]{0:T(1024)} %param.29) | copy-start | bytes 24580
  10.9 0.7 %copy-start.8 = (bf16[16,128]{1,0:T(8,128)(2,1)S(1)}, bf16[16,128]{1,0:T(8,128)(2,1)}, u32[]{:S(2)}) copy-start(bf16[16,128]{1,0:T(8,128)(2,1)} %residual_ref.1) | copy-start | bytes 12292
  11.6 0.7 %copy-start.9 = (bf16[1,8,128]{2,1,0:T(8,128)(2,1)S(1)}, bf16[1,8,128]{2,1,0:T(8,128)(2,1)}, u32[]{:S(2)}) copy-start(bf16[1,8,128]{2,1,0:T(8,128)(2,1)} %q_ref.1) | copy-start | bytes 6148
  12.2 0.7 %copy-start.10 = (bf16[1,2,128]{2,1,0:T(2,128)(2,1)S(1)}, bf16[1,2,128]{2,1,0:T(2,128)(2,1)}, u32[]{:S(2)}) copy-start(bf16[1,2,128]{2,1,0:T(2,128)(2,1)} %fresh_ref.1) | copy-start | bytes 1540
  12.9 0.7 %copy-start.11 = (bf16[1,2,128]{2,1,0:T(2,128)(2,1)S(1)}, bf16[1,2,128]{2,1,0:T(2,128)(2,1)}, u32[]{:S(2)}) copy-start(bf16[1,2,128]{2,1,0:T(2,128)(2,1)} %vnew_ref.1) | copy-start | bytes 1540
  13.6 0.7 %copy-start.12 = (f32[1,8]{1,0:T(1,128)S(1)}, f32[1,8]{1,0:T(1,128)}, u32[]{:S(2)}) copy-start(f32[1,8]{1,0:T(1,128)} %forget_ref.1) | copy-start | bytes 100
where the time goes:
time: 39.5 us; the launch traced here: 38.9 us
  Pallas kernels  24.1 us (61%)
  local copies, waits for them, and re-layouts  14.1 us (36%)
  between operations  0.68 us (2%)
    pallas_call x1, Pallas kernels, on_device(): pl.pallas_call(functools.partial(layer, n), out_shape=jax.ShapeDtypeStruc...  24.1 us
    unnamed x29, local copies, waits for them, and re-layouts  14.1 us

commit v1 on v0

--- a/solution.py
+++ b/solution.py
@@ -11,6 +11,7 @@
 routed_scale = 2.5
 contract_last = (((1,), (1,)), ((), ()))
 LANES = 128
+VMEM_LIMIT = 67043328
 f32 = jnp.float32
 bf16 = jnp.bfloat16
 
@@ -50,14 +51,14 @@
 def layer(
     n,
     lengths_ref,
-    q_ref,
-    fresh_ref,
-    vnew_ref,
-    forget_ref,
-    residual_ref,
-    gain_ref,
-    routes_ref,
-    route_scores_ref,
+    q_hbm,
+    fresh_hbm,
+    vnew_hbm,
+    forget_hbm,
+    residual_hbm,
+    gain_hbm,
+    routes_hbm,
+    route_scores_hbm,
     keys_hbm,
     values_hbm,
     cumlog_hbm,
@@ -69,6 +70,14 @@
     sup_hbm,
     sdown_hbm,
     out_ref,
+    q_ref,
+    fresh_ref,
+    vnew_ref,
+    forget_ref,
+    residual_ref,
+    gain_ref,
+    routes_ref,
+    route_scores_ref,
     keys,
     values,
     cumlog,
@@ -86,6 +95,7 @@
     mid_buf,
     eo_src,
     eo_buf,
+    small_sem,
     load_sem,
     key_sem,
     value_sem,
@@ -119,11 +129,30 @@
     down_copy = pltpu.make_async_copy(down_hbm.at[0], down_w, load_sem.at[6])
     sdown_copy = pltpu.make_async_copy(sdown_hbm, sdown_w, load_sem.at[7])
 
+    smalls = [
+        pltpu.make_async_copy(src, dst, small_sem.at[i])
+        for i, (src, dst) in enumerate(
+            (
+                (q_hbm, q_ref),
+                (fresh_hbm, fresh_ref),
+                (vnew_hbm, vnew_ref),
+                (forget_hbm, forget_ref),
+                (routes_hbm, routes_ref),
+                (route_scores_hbm, route_scores_ref),
+                (residual_hbm, residual_ref),
+                (gain_hbm, gain_ref),
+            )
+        )
+    ]
+    for copy in smalls[:4]:
+        copy.start()
     cumlog_copy.start()
     for c in range(chunks):
         key_copy(c).start()
     for c in range(chunks):
         value_copy(c).start()
+    for copy in smalls[4:]:
+        copy.start()
     out_w_copy.start()
 
     barrier = pltpu.get_barrier_semaphore()
@@ -167,6 +196,8 @@
 
         lax.fori_loop(1, n, one, 0)
 
+    for copy in smalls[:4]:
+        copy.wait()
     inv_root = head_size ** (-0.5)
     length = lengths_ref[0]
     q = q_ref[0]
@@ -231,16 +262,25 @@
     pl.semaphore_wait(barrier, n - 1)
     spread(0, att_buf)
 
+    for copy in smalls[4:]:
+        copy.wait()
     route_scores = route_scores_ref[...]
     gate_weights = (
-        route_scores / jnp.sum(route_scores, axis=1, keepdims=True) * routed_scale
-    )
-    expert_lane = lax.broadcasted_iota(jnp.int32, (rows, n), 1)
-    share = jnp.zeros((rows, n), f32)
-    for k in range(routes_ref.shape[1]):
+        route_scores / jnp.sum(route_scores, axis=0, keepdims=True) * routed_scale
+    )
+    expert_row = lax.broadcasted_iota(jnp.int32, (n, rows), 0)
+    share = jnp.zeros((n, rows), f32)
+    for k in range(routes_ref.shape[0]):
         share = share + jnp.where(
-            routes_ref[:, k : k + 1] == expert_lane, gate_weights[:, k : k + 1], 0.0
+            routes_ref[k : k + 1] == expert_row, gate_weights[k : k + 1], 0.0
         )
+    row_eye = lax.broadcasted_iota(jnp.int32, (rows, rows), 0) == lax.broadcasted_iota(
+        jnp.int32, (rows, rows), 1
+    )
+    shares = [
+        jnp.sum(jnp.where(row_eye, share[e : e + 1], 0.0), axis=1, keepdims=True)
+        for e in range(n)
+    ]
     out_w_copy.wait()
 
     arrive(0, att_buf)
@@ -299,7 +339,7 @@
     total = stream.astype(f32) + jnp.dot(mid, sdown_w[...], preferred_element_type=f32)
     arrive(3, eo_buf)
     for e in range(n):
-        total = total + share[:, e : e + 1] * eo_buf[e][:, :width].astype(f32)
+        total = total + shares[e] * eo_buf[e][:, :width].astype(f32)
     out_ref[...] = total.astype(bf16)
 
     sent(0, att_buf)
@@ -339,7 +379,7 @@
         mid_lanes = -(-shared_gate.shape[0] // LANES) * LANES
         chunks = 4
         vmem = pl.BlockSpec(memory_space=pltpu.VMEM)
-        hbm = pl.BlockSpec(memory_space=pl.ANY)
+        hbm = pl.BlockSpec(memory_space=pltpu.HBM)
 
         def like(a, drop=0):
             return pltpu.VMEM(a.shape[drop:], a.dtype)
@@ -347,9 +387,17 @@
         return pl.pallas_call(
             functools.partial(layer, n),
             out_shape=jax.ShapeDtypeStruct((rows, width), bf16),
-            in_specs=[pl.BlockSpec(memory_space=pltpu.SMEM)] + [vmem] * 8 + [hbm] * 10,
+            in_specs=[pl.BlockSpec(memory_space=pltpu.SMEM)] + [hbm] * 18,
             out_specs=vmem,
             scratch_shapes=[
+                like(queries),
+                like(fresh_token_key),
+                like(value_new),
+                like(forget_logit),
+                like(residual),
+                pltpu.VMEM((1, norm_gain.shape[0]), f32),
+                pltpu.VMEM(routes.shape[::-1], routes.dtype),
+                pltpu.VMEM(route_scores.shape[::-1], f32),
                 like(cache_keys, 1),
                 like(cache_values, 1),
                 like(cache_cumlog, 1),
@@ -368,13 +416,14 @@
                 pltpu.VMEM((n, rows, lanes), bf16),
                 pltpu.VMEM((n, rows, lanes), bf16),
                 pltpu.SemaphoreType.DMA((8,)),
+                pltpu.SemaphoreType.DMA((8,)),
                 pltpu.SemaphoreType.DMA((chunks,)),
                 pltpu.SemaphoreType.DMA((chunks,)),
                 pltpu.SemaphoreType.DMA((4, n)),
                 pltpu.SemaphoreType.DMA((4, n)),
             ],
             compiler_params=pltpu.CompilerParams(
-                collective_id=0, has_side_effects=True, vmem_limit_bytes=48 * 1024 * 1024
+                collective_id=0, has_side_effects=True, vmem_limit_bytes=VMEM_LIMIT
             ),
             name="layer",
         )(
@@ -385,8 +434,8 @@
             forget_logit,
             residual,
             norm_gain.reshape(1, -1),
-            routes,
-            route_scores,
+            routes.T,
+            route_scores.T,
             cache_keys,
             cache_values,
             cache_cumlog,

time: 39.5 us -> 27.2 us (0.69)
  local copies, waits for them, and re-layouts: 14.1 us -> 1.28 us
  Pallas kernels: 24.1 us -> 25.1 us
    unnamed x29 -> x1, local copies, waits for them, and re-layouts: 14.1 us -> 1.28 us
    pallas_call x1, Pallas kernels: 24.1 us -> 25.1 us  [on_device(): pl.pallas_call(functools.partial(layer, n), out_shape=jax.ShapeDtypeStruc...]
where the time goes in v1:
time: 27.2 us; the launch traced here: 27 us
  Pallas kernels  25.1 us (92%)
  local copies, waits for them, and re-layouts  1.28 us (5%)
  between operations  0.66 us (2%)
    pallas_call x1, Pallas kernels, on_device(): pl.pallas_call(functools.partial(layer, n), out_shape=jax.ShapeDtypeStruc...  25.1 us
    unnamed x1, local copies, waits for them, and re-layouts  1.28 us

profile of v1, /device:TPU:0, one launch (start us, length us, event | category | flops | bytes accessed | tf_op | source)
XLA Modules:
  0.0 27.0 jit_solution(3770881317004649861)
XLA Ops:
  0.7 25.1 %layer.1 = bf16[16,128]{1,0:T(8,128)(2,1)} custom-call(s32[1]{0:T(128)S(6)} %copy.21.lengths_ref, bf16[1,8,128]{2,1,0:T(8,128)(2,1)} %q_hbm.1, bf16[1,2,128]{2,1,0:T(2,128)(2,1)} %fresh_hbm.1, bf16[1,2,128]{2,1,0:T(2,128)(2,1)} %vnew_hbm.1, f32[1,8]{1,0:T(1,128)} %forget_hbm.1, bf16[16,128]{1,0:T(8,128)(2,1)} %residual_hbm.1, f32[1,2048]{1,0:T(1,128)} %bitcast.3, ...), custom_call_target="tpu_custom_call" | custom-call | tf_op jit(solution)/shard_map/layer/pallas_call | solution.py:387
  25.7 1.3 %copy.22 = bf16[16,128]{1,0:T(8,128)(2,1)} copy(bf16[16,128]{1,0:T(8,128)(2,1)} %layer.1) | data formatting | bytes 8192

commit v2 on v1

--- a/solution.py
+++ b/solution.py
@@ -172,9 +172,18 @@
             device_id={"ep": peer},
         )
 
+    wide = max(width, 2 * LANES)
+    per = wide // width
+    turns = model // wide
+    home = me // per
+    toward = 1 - 2 * (home // (turns // 2))
+
+    def visit(i):
+        return lax.rem(home + toward * i + turns, turns)
+
     def spread(phase, buf):
         def one(i, carry):
-            peer = lax.rem(me + i, n)
+            peer = lax.rem(me + toward * (n - i) + n, n)
             remote(phase, buf.at[me], buf.at[me], peer, me).start()
             return carry
 
@@ -296,30 +305,40 @@
     sup_copy.wait()
     gate_copy.wait()
     up_copy.wait()
-    arrive(1, stream_buf)
-
-    full = join_lanes([stream_buf[j] for j in range(n)], width).astype(f32)
-    inv_rms = lax.rsqrt(jnp.mean(full * full, axis=1, keepdims=True) + norm_eps)
-    normed = (full * inv_rms * gain_ref[...]).astype(bf16)
-
-    def hidden_of(gate, up):
-        gated = dot_t(normed, gate)
-        return (jax.nn.silu(gated) * dot_t(normed, up)).astype(bf16)
-
-    mid_buf[me] = widen(hidden_of(sgate_w[...], sup_w[...]))
+
+    def here(peer):
+        remote(1, stream_buf.at[peer], stream_buf.at[peer], peer, peer).wait_recv()
+
+    weights = (sgate_w, sup_w, gate_w, up_w)
+    sums = [jnp.zeros((rows, w.shape[0]), f32) for w in weights]
+    squares = jnp.zeros((rows, 1), f32)
+    for i in range(turns):
+        c = visit(i)
+        part = pl.ds(pl.multiple_of(c * wide, wide), wide)
+        for t in range(per):
+            peer = c * per + t
+            if i:
+                here(peer)
+            else:
+                pl.when(peer != me)(functools.partial(here, peer))
+        block = join_lanes([stream_buf[c * per + t] for t in range(per)], width).astype(f32)
+        squares = squares + jnp.sum(block * block, axis=1, keepdims=True)
+        scaled = (block * gain_ref[:, part]).astype(bf16)
+        sums = [total + dot_t(scaled, w[:, part]) for total, w in zip(sums, weights)]
+    inv_rms = lax.rsqrt(squares * (1.0 / model) + norm_eps)
+    sgated, supped, gated, upped = [total * inv_rms for total in sums]
+
+    mid_buf[me] = widen((jax.nn.silu(sgated) * supped).astype(bf16))
     spread(2, mid_buf)
 
-    hidden = hidden_of(gate_w[...], up_w[...])
+    hidden = (jax.nn.silu(gated) * upped).astype(bf16)
     down_copy.wait()
-    wide = max(width, 2 * LANES)
-    per = wide // width
-    turns = model // wide
 
     def send_block(peer):
         remote(3, eo_src.at[peer], eo_buf.at[me], peer, me).start()
 
     for i in range(turns):
-        c = lax.rem(me // per + 1 + i, turns)
+        c = visit(turns - 1 - i)
         part = pl.ds(pl.multiple_of(c * wide, wide), wide)
         out = jnp.dot(hidden, down_w[:, part], preferred_element_type=f32).astype(bf16)
         for s in range(per):

time: 27.2 us -> 26.6 us (0.978)
  Pallas kernels: 25.1 us -> 24.4 us
    pallas_call x1, Pallas kernels: 25.1 us -> 24.4 us  [on_device(): pl.pallas_call(functools.partial(layer, n), out_shape=jax.ShapeDtypeStruc...]
where the time goes in v2:
time: 26.6 us; the launch traced here: 26.4 us
  Pallas kernels  24.4 us (92%)
  local copies, waits for them, and re-layouts  1.28 us (5%)
  between operations  0.66 us (2%)
    pallas_call x1, Pallas kernels, on_device(): pl.pallas_call(functools.partial(layer, n), out_shape=jax.ShapeDtypeStruc...  24.4 us
    unnamed x1, local copies, waits for them, and re-layouts  1.28 us

profile of v2, /device:TPU:0, one launch (start us, length us, event | category | flops | bytes accessed | tf_op | source)
XLA Modules:
  0.0 26.4 jit_solution(12765121696995113914)
XLA Ops:
  0.7 24.4 %layer.1 = bf16[16,128]{1,0:T(8,128)(2,1)} custom-call(s32[1]{0:T(128)S(6)} %copy.21.lengths_ref, bf16[1,8,128]{2,1,0:T(8,128)(2,1)} %q_hbm.1, bf16[1,2,128]{2,1,0:T(2,128)(2,1)} %fresh_hbm.1, bf16[1,2,128]{2,1,0:T(2,128)(2,1)} %vnew_hbm.1, f32[1,8]{1,0:T(1,128)} %forget_hbm.1, bf16[16,128]{1,0:T(8,128)(2,1)} %residual_hbm.1, f32[1,2048]{1,0:T(1,128)} %bitcast.3, ...), custom_call_target="tpu_custom_call" | custom-call | tf_op jit(solution)/shard_map/layer/pallas_call | solution.py:406
  25.1 1.3 %copy.22 = bf16[16,128]{1,0:T(8,128)(2,1)} copy(bf16[16,128]{1,0:T(8,128)(2,1)} %layer.1) | data formatting | bytes 8192
